TPU v7x, 512 devices: a whole 4x8x8 slice. The times are simulated.
512 devices in a mesh: fs: 64 (over z, y), tp: 8 (over x, core).
Axes of the slice: x: 4, y: 8, z: 8, core: 2. Of those that a mesh axis runs over, the one named last changes fastest.
Arguments:
- inputs: bfloat16 [32768, 2048], P('fs', 'tp'), may hold values from -6 to 6
- value_cotangent: bfloat16 [32768, 2048], P('fs', 'tp'), may hold values from -6 to 6
- first_map: bfloat16 [32768, 2048], P('fs', 'tp'), may hold values from -6 to 6
- second_map: bfloat16 [32768, 2048], P('fs', 'tp'), may hold values from -6 to 6
- lambdas: float32 [16], P('tp'), may hold values from 0.3 to 0.8
- head_gain: float32 [128], replicated, may hold values from 0.1 to 1.9
- output_cotangent: bfloat16 [32768, 2048], P('fs', 'tp'), may hold values from -6 to 6
- value_factor: bfloat16 [2048, 256], replicated, may hold values from -0.125 to 0.125
- output_factor: bfloat16 [2048, 256], replicated, may hold values from -0.125 to 0.125
- value_weight: float32 [2048, 2048], P('fs', 'tp'), may hold values from -0.125 to 0.125
- output_weight: float32 [2048, 2048], P('tp', 'fs'), may hold values from -0.125 to 0.125
- value_moment: float32 [256, 2048], P('fs', 'tp'), may hold values from -6 to 6
- value_second: float32 [256, 2048], P('fs', 'tp'), may hold values from 0.25 to 4
- output_moment: float32 [256, 2048], P('fs', 'tp'), may hold values from -6 to 6
- output_second: float32 [256, 2048], P('fs', 'tp'), may hold values from 0.25 to 4
Outputs:
- value_master: float32 [2048, 2048], P('fs', 'tp')
- output_master: float32 [2048, 2048], P('tp', 'fs')
- value_moment_new: float32 [256, 2048], P('fs', 'tp')
- value_second_new: float32 [256, 2048], P('fs', 'tp')
- output_moment_new: float32 [256, 2048], P('fs', 'tp')
- output_second_new: float32 [256, 2048], P('fs', 'tp')
- value_copy: bfloat16 [2048, 2048], P(None, 'tp')
- output_copy: bfloat16 [2048, 2048], P('tp')
All inputs are finite; a program needn't handle non-finite values.
Results may differ from a plain program's by a relative error of at most 0.0027.
Values may be sent and summed in bfloat16 or wider, within the bound.
No kernel may reach another device: no remote copies, remote signals or barrier semaphores. Data moves between devices by JAX's collectives and lax.ppermute only.
A program may use at most 64 MiB of HBM per device.

v0:
```python
import math
import jax
import jax.numpy as jnp
from jax import lax
from jax.sharding import PartitionSpec as P

F32 = jnp.float32
BF16 = jnp.bfloat16
F16 = jnp.float16
WEIGHT_SCALE = 2.0**18
TOKEN_SCALE = 2.0**4
LOW_SCALE = 2.0 ** (-2)
DIRECTION_SCALE = 2.0**8


def dot(left, right, left_dim, right_dim):
    return lax.dot_general(
        left, right, (((left_dim,), (right_dim,)), ((), ())), preferred_element_type=F32
    )


def two_parts(x):
    high = lax.reduce_precision(x, 8, 7)
    return (high.astype(BF16), (x - high).astype(BF16))


def dot_two(left, right_parts, left_dim, right_dim):
    high, low = right_parts
    return dot(left, high, left_dim, right_dim) + dot(left, low, left_dim, right_dim)


def copy_for_each(x, axis):
    size = lax.axis_size(axis)
    return lax.all_to_all(jnp.broadcast_to(x[None], (size, *x.shape)), axis, 0, 0, tiled=True)


def normed_heads(first_map, second_map, lambdas, head_gain):
    width = head_gain.shape[0]
    heads = []
    for h in range(lambdas.shape[0]):
        cols = slice(h * width, (h + 1) * width)
        difference = first_map[:, cols].astype(F32) - lambdas[h] * second_map[:, cols].astype(F32)
        mean = jnp.mean(difference * difference, axis=-1, keepdims=True)
        heads.append((difference * lax.rsqrt(mean + 1e-06) * head_gain[None, :]).astype(BF16))
    return jnp.concatenate(heads, axis=1)


def local(
    inputs,
    value_cotangent,
    first_map,
    second_map,
    lambdas,
    head_gain,
    output_cotangent,
    value_factor,
    output_factor,
    value_weight,
    output_weight,
    value_moment,
    value_second,
    output_moment,
    output_second,
):
    tok_rows, cols = inputs.shape
    rank = value_factor.shape[1]
    fs_size, tp_size = (lax.axis_size("fs"), lax.axis_size("tp"))
    fs_index, tp_index = (lax.axis_index("fs"), lax.axis_index("tp"))
    width_rows = value_weight.shape[0]
    own_weights = jnp.concatenate([value_weight, output_weight.T], axis=1)
    weights = lax.all_gather((own_weights * WEIGHT_SCALE).astype(F16), "fs", axis=0, tiled=True)
    in_rows = lax.dynamic_slice_in_dim(value_factor, tp_index * cols, cols, 0)
    cot_rows = lax.dynamic_slice_in_dim(output_factor, tp_index * cols, cols, 0)
    projected = jnp.concatenate(
        [dot(inputs, in_rows, 1, 0), dot(output_cotangent, cot_rows, 1, 0)], axis=1
    )
    pieces = (projected * TOKEN_SCALE).astype(F16).reshape(tp_size, -1, 2 * rank)
    pieces = lax.all_to_all(pieces, "tp", 0, 0, tiled=True)
    summed = jnp.sum(pieces.astype(F32), axis=0).astype(F16)
    tokens = copy_for_each(summed, "tp").reshape(tok_rows, 2 * rank).astype(F32)
    heads_out = normed_heads(first_map, second_map, lambdas, head_gain)
    scale = LOW_SCALE / (TOKEN_SCALE * math.sqrt(tok_rows * fs_size))
    token_parts = two_parts(tokens)
    low_value = dot_two(value_cotangent, [p[:, :rank] for p in token_parts], 0, 0)
    low_output = dot_two(heads_out, [p[:, rank:] for p in token_parts], 0, 0)
    partial = jnp.concatenate([low_value.T, low_output.T], axis=1) * scale
    tiles = partial.astype(F16).reshape(fs_size, -1, 2 * cols)
    tiles = lax.all_to_all(tiles, "fs", 0, 0, tiled=True)
    own_rows = jnp.sum(tiles.astype(F32), axis=0) * (1.0 / LOW_SCALE)
    moments = jnp.concatenate([value_moment, output_moment], axis=1)
    seconds = jnp.concatenate([value_second, output_second], axis=1)
    moment_new = 0.8 * moments + 0.2 * own_rows
    second_new = 0.95 * seconds + 0.05 * own_rows * own_rows
    direction = moment_new / (jnp.sqrt(second_new) + 1e-08)
    directions = copy_for_each((direction * DIRECTION_SCALE).astype(F16), "fs")
    parts = two_parts(directions.reshape(rank, 2 * cols).astype(F32))
    value_parts = [p[:, :cols] for p in parts]
    output_parts = [p[:, cols:] for p in parts]
    rate = 0.05 / DIRECTION_SCALE
    value_rows = lax.dynamic_slice_in_dim(value_factor, fs_index * width_rows, width_rows, 0)
    output_rows = lax.dynamic_slice_in_dim(output_factor, fs_index * width_rows, width_rows, 0)
    value_master = value_weight - rate * dot_two(value_rows, value_parts, 1, 0)
    output_master = output_weight - rate * dot_two(output_rows, output_parts, 1, 0).T
    old_value = weights[:, :cols].astype(F32) * (1.0 / WEIGHT_SCALE)
    old_output = weights[:, cols:].T.astype(F32) * (1.0 / WEIGHT_SCALE)
    value_copy = (old_value - rate * dot_two(value_factor, value_parts, 1, 0)).astype(BF16)
    step_output = dot(output_parts[0], output_factor, 0, 1) + dot(
        output_parts[1], output_factor, 0, 1
    )
    output_copy = (old_output - rate * step_output).astype(BF16)
    return (
        value_master,
        output_master,
        moment_new[:, :cols],
        second_new[:, :cols],
        moment_new[:, cols:],
        second_new[:, cols:],
        value_copy,
        output_copy,
    )


def solution(mesh):
    in_specs = (
        P("fs", "tp"),
        P("fs", "tp"),
        P("fs", "tp"),
        P("fs", "tp"),
        P("tp"),
        P(),
        P("fs", "tp"),
        P(),
        P(),
        P("fs", "tp"),
        P("tp", "fs"),
        P("fs", "tp"),
        P("fs", "tp"),
        P("fs", "tp"),
        P("fs", "tp"),
    )
    out_specs = (
        P("fs", "tp"),
        P("tp", "fs"),
        P("fs", "tp"),
        P("fs", "tp"),
        P("fs", "tp"),
        P("fs", "tp"),
        P(None, "tp"),
        P("tp", None),
    )
    return jax.shard_map(local, mesh=mesh, in_specs=in_specs, out_specs=out_specs, check_vma=False)
```

profile of v0, /device:TPU:8, one launch (start us, length us, event | category | flops | bytes accessed | tf_op | source)
XLA Modules:
  0.0 144.4 jit_solution(10989713373295257813)
XLA Ops:
  0.6 0.0 copy-start
  0.6 0.0 copy-start.6
  0.7 1.2 copy-done
  1.9 1.2 convolution_bitcast_fusion.1
  3.1 0.2 copy.31
  3.3 0.0 copy-done.6
  3.3 0.0 copy-start.13
  3.3 0.0 copy-start.7
  3.3 0.0 copy-start.8
  3.3 1.2 convolution_bitcast_fusion
  4.5 0.0 copy-start.3
  4.5 0.0 copy-start.4
  4.5 0.2 copy.32
  4.7 0.9 fusion.12
  5.6 4.4 %all-to-all-start = ((f16[8,64,512]{2,1,0:T(8,128)(2,1)}), f16[8,64,512]{2,1,0:T(8,128)(2,1)S(1)}, u32[]{:S(2)}, u32[]{:S(2)}) async-start(f16[8,64,512]{2,1,0:T(8,128)(2,1)} %fusion.12), calls=%async_computation | async-start | bytes 1048576 | tf_op jit(solution)/shard_map/all_to_all | solution.py:78
  10.1 0.0 copy-done.13
  10.1 0.6 fusion.55
  10.7 0.0 copy-done.7
  10.7 1.5 %multiply_reduce_fusion.1 = (f32[512]{0:T(512)S(1)}, f32[512]{0:T(512)S(1)}) fusion(f32[]{:T(128)} %bitcast.6, bf16[512,256]{1,0:T(8,128)(2,1)S(1)} %copy-done.3, bf16[512,256]{1,0:T(8,128)(2,1)S(1)} %copy-done.4, f32[]{:T(128)} %bitcast.7), kind=kLoop, calls=%fused_computation.42 | loop fusion | flops 785408 | bytes 528392 | tf_op jit(solution)/shard_map/reduce_sum | solution.py:43
  12.2 8.2 %all-to-all-done = f16[8,64,512]{2,1,0:T(8,128)(2,1)S(1)} async-done(((f16[8,64,512]{2,1,0:T(8,128)(2,1)}), f16[8,64,512]{2,1,0:T(8,128)(2,1)S(1)}, u32[]{:S(2)}, u32[]{:S(2)}) %all-to-all-start) | async-done | bytes 524320 | tf_op jit(solution)/shard_map/all_to_all | solution.py:78
  20.4 0.1 convert_reduce_fusion
  20.5 0.8 broadcast_in_dim.4
  21.3 3.5 %all-to-all-start.1 = ((f16[8,64,512]{2,1,0:T(8,128)(2,1)}), f16[8,64,512]{2,1,0:T(8,128)(2,1)S(1)}, u32[]{:S(2)}, u32[]{:S(2)}) async-start(f16[8,64,512]{2,1,0:T(8,128)(2,1)} %broadcast_in_dim.4), calls=%async_computation.1 | async-start | bytes 1048576 | tf_op jit(solution)/shard_map/all_to_all | solution.py:34
  24.9 1.5 %multiply_convert_fusion.1 = (bf16[512,128]{1,0:T(8,128)(2,1)S(1)}, bf16[512,128]{1,0:T(8,128)(2,1)S(1)}) fusion(f32[128]{0:T(128)S(1)} %copy-done.14, f32[512]{0:T(512)S(1)} %get-tuple-element.52, f32[]{:T(128)} %bitcast.6, bf16[512,256]{1,0:T(8,128)(2,1)S(1)} %copy-done.3, bf16[512,256]{1,0:T(8,128)(2,1)S(1)} %copy-done.4, f32[512]{0:T(512)S(1)} %get-tuple-element.51, ...), kind=kLoop, calls=%fused_computation.41 | loop fusion | flops 917504 | bytes 791048 | tf_op jit(solution)/shard_map/convert_element_type | solution.py:44
  26.4 0.0 copy-start.5
  26.4 8.7 %all-to-all-done.1 = f16[8,64,512]{2,1,0:T(8,128)(2,1)S(1)} async-done(((f16[8,64,512]{2,1,0:T(8,128)(2,1)}), f16[8,64,512]{2,1,0:T(8,128)(2,1)S(1)}, u32[]{:S(2)}, u32[]{:S(2)}) %all-to-all-start.1) | async-done | bytes 524320 | tf_op jit(solution)/shard_map/all_to_all | solution.py:34
  35.1 0.2 fusion.11
  35.3 0.3 fusion.16
  35.5 0.3 convolution_add_fusion.2
  35.8 0.1 concatenate.42
  35.9 0.0 copy-done.5
  35.9 0.3 fusion.19
  36.2 0.3 convolution_add_fusion.3
  36.4 0.0 copy-start.9
  36.5 0.0 copy-start.10
  36.5 0.0 copy-start.11
  36.5 0.0 copy-start.12
  36.5 0.1 concatenate.40
  36.6 0.9 fusion.14
  37.4 16.6 %all-to-all-start.2 = ((f16[64,4,512]{2,1,0:T(4,128)(2,1)}), f16[64,4,512]{2,1,0:T(4,128)(2,1)S(1)}, u32[]{:S(2)}, u32[]{:S(2)}) async-start(f16[64,4,512]{2,1,0:T(4,128)(2,1)} %fusion.14), calls=%async_computation.2 | async-start | bytes 524288 | tf_op jit(solution)/shard_map/all_to_all | solution.py:88
  54.0 52.9 %all-gather.1 = f16[2048,512]{1,0:T(8,128)(2,1)S(1)} all-gather(f16[32,512]{1,0:T(8,128)(2,1)S(1)} %fusion.35), channel_id=1, replica_groups=mesh['fs'=64,'tp'=8] {'fs'}, dimensions={0}, use_global_device_ids=true | all-gather | bytes 2129920 | tf_op jit(solution)/shard_map/all_gather | solution.py:71
  106.9 0.0 all-to-all-done.2
  106.9 0.1 convert_reduce_fusion.1
  107.1 0.8 broadcast_in_dim.5
  107.9 10.6 %all-to-all-start.3 = ((f16[64,4,512]{2,1,0:T(4,128)(2,1)}), f16[64,4,512]{2,1,0:T(4,128)(2,1)S(1)}, u32[]{:S(2)}, u32[]{:S(2)}) async-start(f16[64,4,512]{2,1,0:T(4,128)(2,1)} %broadcast_in_dim.5), calls=%async_computation.3 | async-start | bytes 524288 | tf_op jit(solution)/shard_map/all_to_all | solution.py:34
  118.5 1.8 %fusion.52 = (f16[2048,256]{1,0:T(8,128)(2,1)}, f16[2048,256]{1,0:T(8,128)(2,1)}) fusion(f16[2048,512]{1,0:T(8,128)(2,1)S(1)} %all-gather.1), kind=kLoop, calls=%fused_computation.80 | loop fusion | bytes 4194304 | tf_op jit(solution)/shard_map/slice | solution.py:105
  120.3 2.6 %copy.37 = f16[2048,256]{0,1:T(8,128)(2,1)} copy(f16[2048,256]{1,0:T(8,128)(2,1)} %get-tuple-element.37) | data formatting | bytes 2097152
  122.9 1.7 %copy.36 = f16[2048,256]{0,1:T(8,128)(2,1)} copy(f16[2048,256]{1,0:T(8,128)(2,1)S(1)} %copy-done.2) | data formatting | bytes 2097152
  124.6 0.6 fusion.53
  125.2 0.6 fusion.54
  125.8 5.8 %all-to-all-done.3 = f16[64,4,512]{2,1,0:T(4,128)(2,1)S(1)} async-done(((f16[64,4,512]{2,1,0:T(4,128)(2,1)}), f16[64,4,512]{2,1,0:T(4,128)(2,1)S(1)}, u32[]{:S(2)}, u32[]{:S(2)}) %all-to-all-start.3) | async-done | bytes 262176 | tf_op jit(solution)/shard_map/all_to_all | solution.py:34
  131.6 0.1 convert_element_type.112
  131.7 0.2 reshape.92
  131.9 0.1 fusion.13
  132.0 1.7 %fusion.25 = f32[256,2048]{1,0:T(8,128)S(1)} fusion(bf16[2048,256]{1,0:T(8,128)(2,1)} %param.23, bf16[256,512]{1,0:T(8,128)(2,1)S(1)} %get-tuple-element.42), kind=kOutput, calls=%fused_computation.48 | convolution fusion | flops 268435456 | bytes 3276800 | tf_op jit(solution)/shard_map/dot_general | solution.py:17
  133.7 0.0 copy-start.1
  133.7 0.5 fusion.31
  134.2 0.9 fusion.27
  135.0 0.1 fusion.33
  135.2 1.6 %fusion.5 = bf16[2048,256]{0,1:T(8,128)(2,1)} fusion(f32[256,2048]{1,0:T(8,128)S(1)} %fusion.31, bf16[2048,256]{1,0:T(8,128)(2,1)S(1)} %copy-done, f16[2048,256]{0,1:T(8,128)(2,1)S(1)} %copy-done.1, bf16[256,512]{1,0:T(8,128)(2,1)S(1)} %get-tuple-element.41), kind=kOutput, calls=%fused_computation.7 | convolution fusion | flops 271581184 | bytes 5373952 | tf_op jit(solution)/shard_map/dot_general | solution.py:17
  136.8 2.3 %copy.35 = bf16[2048,256]{1,0:T(8,128)(2,1)} copy(bf16[2048,256]{0,1:T(8,128)(2,1)} %fusion.5) | data formatting | bytes 2097152
  139.1 1.5 %fusion.8 = f32[256,32]{0,1:T(8,128)} fusion(f32[256,32]{0,1:T(8,128)S(1)} %copy-done.7, f32[256,32]{0,1:T(8,128)S(1)} %fusion.27, bf16[256,512]{1,0:T(8,128)(2,1)S(1)} %get-tuple-element.41, bf16[2048,256]{1,0:T(8,128)(2,1)} %param.23, s32[]{:T(128)S(6)} %select_n.8), kind=kOutput, calls=%fused_computation.17 | convolution fusion | flops 4218880 | bytes 245764 | tf_op jit(solution)/shard_map/dot_general | solution.py:17
  140.6 0.8 fusion.10
  141.3 3.1 %fusion.6 = bf16[256,2048]{1,0:T(8,128)(2,1)} fusion(f32[256,2048]{1,0:T(8,128)S(1)} %fusion.25, bf16[2048,256]{1,0:T(8,128)(2,1)} %param.23, f16[2048,256]{0,1:T(8,128)(2,1)} %copy.37, bf16[256,512]{1,0:T(8,128)(2,1)S(1)} %get-tuple-element.41), kind=kOutput, calls=%fused_computation.8 | convolution fusion | flops 271581184 | bytes 5373952 | tf_op jit(solution)/shard_map/dot_general | solution.py:17
  (16 shorter events, 0.1 us)
Async XLA Ops:
  0.6 1.2 copy-start
  0.6 2.6 %copy-start.6 = (bf16[512,256]{1,0:T(8,128)(2,1)S(1)}, bf16[512,256]{1,0:T(8,128)(2,1)}, u32[]{:S(2)}) copy-start(bf16[512,256]{1,0:T(8,128)(2,1)} %param.21) | copy-start | bytes 786436
  3.3 6.8 %copy-start.13 = (f32[2]{0:T(128)S(1)}, f32[2]{0:T(128)}, u32[]{:S(2)}) copy-start(f32[2]{0:T(128)} %param.19) | copy-start | bytes 28
  3.3 7.4 %copy-start.7 = (f32[256,32]{0,1:T(8,128)S(1)}, f32[256,32]{0,1:T(8,128)}, u32[]{:S(2)}) copy-start(f32[256,32]{0,1:T(8,128)} %param.25) | copy-start | bytes 98308
  3.3 7.3 %copy-start.8 = (f32[32,256]{1,0:T(8,128)S(1)}, f32[32,256]{1,0:T(8,128)}, u32[]{:S(2)}) copy-start(f32[32,256]{1,0:T(8,128)} %param.24) | copy-start | bytes 98308
  4.5 6.2 %copy-start.3 = (bf16[512,256]{1,0:T(8,128)(2,1)S(1)}, bf16[512,256]{1,0:T(8,128)(2,1)}, u32[]{:S(2)}) copy-start(bf16[512,256]{1,0:T(8,128)(2,1)} %param.18) | copy-start | bytes 786436
  4.5 6.2 %copy-start.4 = (bf16[512,256]{1,0:T(8,128)(2,1)S(1)}, bf16[512,256]{1,0:T(8,128)(2,1)}, u32[]{:S(2)}) copy-start(bf16[512,256]{1,0:T(8,128)(2,1)} %param.17) | copy-start | bytes 786436
  5.6 19.2 %copy-start.14 = (f32[128]{0:T(128)S(1)}, f32[128]{0:T(128)}, u32[]{:S(2)}) copy-start(f32[128]{0:T(128)} %param.20) | copy-start | bytes 1540
  5.6 14.7 %all-to-all-start = ((f16[8,64,512]{2,1,0:T(8,128)(2,1)}), f16[8,64,512]{2,1,0:T(8,128)(2,1)S(1)}, u32[]{:S(2)}, u32[]{:S(2)}) async-start(f16[8,64,512]{2,1,0:T(8,128)(2,1)} %fusion.12), calls=%async_computation | async-start | bytes 1048576 | tf_op jit(solution)/shard_map/all_to_all | solution.py:78
  21.3 13.7 %all-to-all-start.1 = ((f16[8,64,512]{2,1,0:T(8,128)(2,1)}), f16[8,64,512]{2,1,0:T(8,128)(2,1)S(1)}, u32[]{:S(2)}, u32[]{:S(2)}) async-start(f16[8,64,512]{2,1,0:T(8,128)(2,1)} %broadcast_in_dim.4), calls=%async_computation.1 | async-start | bytes 1048576 | tf_op jit(solution)/shard_map/all_to_all | solution.py:34
  26.4 9.5 %copy-start.5 = (bf16[512,256]{1,0:T(8,128)(2,1)S(1)}, bf16[512,256]{1,0:T(8,128)(2,1)}, u32[]{:S(2)}) copy-start(bf16[512,256]{1,0:T(8,128)(2,1)} %param.16) | copy-start | bytes 786436
  36.4 70.6 %copy-start.9 = (f32[4,256]{1,0:T(4,128)S(1)}, f32[4,256]{1,0:T(4,128)}, u32[]{:S(2)}) copy-start(f32[4,256]{1,0:T(4,128)} %param.29) | copy-start | bytes 12292
  36.5 70.6 %copy-start.10 = (f32[4,256]{1,0:T(4,128)S(1)}, f32[4,256]{1,0:T(4,128)}, u32[]{:S(2)}) copy-start(f32[4,256]{1,0:T(4,128)} %param.27) | copy-start | bytes 12292
  36.5 70.6 %copy-start.11 = (f32[4,256]{1,0:T(4,128)S(1)}, f32[4,256]{1,0:T(4,128)}, u32[]{:S(2)}) copy-start(f32[4,256]{1,0:T(4,128)} %param.28) | copy-start | bytes 12292
  36.5 70.6 %copy-start.12 = (f32[4,256]{1,0:T(4,128)S(1)}, f32[4,256]{1,0:T(4,128)}, u32[]{:S(2)}) copy-start(f32[4,256]{1,0:T(4,128)} %param.26) | copy-start | bytes 12292
  37.4 69.5 %all-to-all-start.2 = ((f16[64,4,512]{2,1,0:T(4,128)(2,1)}), f16[64,4,512]{2,1,0:T(4,128)(2,1)S(1)}, u32[]{:S(2)}, u32[]{:S(2)}) async-start(f16[64,4,512]{2,1,0:T(4,128)(2,1)} %fusion.14), calls=%async_computation.2 | async-start | bytes 524288 | tf_op jit(solution)/shard_map/all_to_all | solution.py:88
  107.9 23.7 %all-to-all-start.3 = ((f16[64,4,512]{2,1,0:T(4,128)(2,1)}), f16[64,4,512]{2,1,0:T(4,128)(2,1)S(1)}, u32[]{:S(2)}, u32[]{:S(2)}) async-start(f16[64,4,512]{2,1,0:T(4,128)(2,1)} %broadcast_in_dim.5), calls=%async_computation.3 | async-start | bytes 524288 | tf_op jit(solution)/shard_map/all_to_all | solution.py:34
  120.3 2.6 %copy-start.2 = (f16[2048,256]{1,0:T(8,128)(2,1)S(1)}, f16[2048,256]{1,0:T(8,128)(2,1)}, u32[]{:S(2)}) copy-start(f16[2048,256]{1,0:T(8,128)(2,1)} %get-tuple-element.38) | copy-start | bytes 3145732
  133.7 1.5 %copy-start.1 = (f16[2048,256]{0,1:T(8,128)(2,1)S(1)}, f16[2048,256]{0,1:T(8,128)(2,1)}, u32[]{:S(2)}) copy-start(f16[2048,256]{0,1:T(8,128)(2,1)} %copy.36) | copy-start | bytes 3145732
where the time goes:
time: 145 us; the launch traced here: 144 us
  blocking collectives  52.9 us (36%)
  starting transfers between devices  35.1 us (24%)
  waiting for transfers between devices  22.7 us (16%)
  local copies, waits for them, and re-layouts  13.7 us (9%)
  matrix products  13.7 us (9%)
  other arithmetic  5.39 us (4%)
    all_gather x1, blocking collectives, local(): lax.all_gather((own_weights * WEIGHT_SCALE).astype(F16), 'fs', axis=0, ti...  52.9 us
    all_to_all x1, starting transfers between devices, local(): tiles = lax.all_to_all(tiles, 'fs', 0, 0, tiled=True)  16.6 us
    all_to_all x2, waiting for transfers between devices, copy_for_each(): lax.all_to_all(jnp.broadcast_to(x[None], (size, *x.shape)), axis, 0, 0, t...  14.5 us
    all_to_all x2, starting transfers between devices, copy_for_each(): lax.all_to_all(jnp.broadcast_to(x[None], (size, *x.shape)), axis, 0, 0, t...  14.1 us
    dot_general x14, matrix products, dot(): lax.dot_general(left, right, (((left_dim,), (right_dim,)), ((), ())), pre...  13.7 us
    all_to_all x1, waiting for transfers between devices, local(): pieces = lax.all_to_all(pieces, 'tp', 0, 0, tiled=True)  8.17 us
    unnamed x33, local copies, waits for them, and re-layouts  7.84 us
    all_to_all x1, starting transfers between devices, local(): pieces = lax.all_to_all(pieces, 'tp', 0, 0, tiled=True)  4.43 us
  transfers between devices with their start and end apart: 4, of which 3 were waited for; matrix products, arithmetic and copies ran while one was open for 8% of the time, Pallas kernels for 0%

commit v1 on v0

--- a/solution.py
+++ b/solution.py
@@ -11,6 +11,11 @@
 TOKEN_SCALE = 2.0**4
 LOW_SCALE = 2.0 ** (-2)
 DIRECTION_SCALE = 2.0**8
+
+
+def gather_from_all(shard, axis, dim):
+    copies = jnp.concatenate([shard] * lax.axis_size(axis), axis=dim)
+    return lax.all_to_all(copies, axis, dim, dim, tiled=True)
 
 
 def dot(left, right, left_dim, right_dim):
@@ -68,7 +73,7 @@
     fs_index, tp_index = (lax.axis_index("fs"), lax.axis_index("tp"))
     width_rows = value_weight.shape[0]
     own_weights = jnp.concatenate([value_weight, output_weight.T], axis=1)
-    weights = lax.all_gather((own_weights * WEIGHT_SCALE).astype(F16), "fs", axis=0, tiled=True)
+    weights = gather_from_all((own_weights * WEIGHT_SCALE).astype(F16), "fs", 0)
     in_rows = lax.dynamic_slice_in_dim(value_factor, tp_index * cols, cols, 0)
     cot_rows = lax.dynamic_slice_in_dim(output_factor, tp_index * cols, cols, 0)
     projected = jnp.concatenate(

time: 145 us -> 170 us (1.17)
  waiting for transfers between devices: 22.7 us -> 78.6 us
  blocking collectives: 52.9 us -> 0 us
  matrix products: 13.7 us -> 20.7 us
  local copies, waits for them, and re-layouts: 13.7 us -> 20.7 us
  other arithmetic: 5.39 us -> 12 us
    all_gather x1 -> x0, blocking collectives: 52.9 us -> none  [local(): lax.all_gather((own_weights * WEIGHT_SCALE).astype(F16), 'fs', axis=0, ti...]
    all_to_all x0 -> x1, waiting for transfers between devices: none -> 37.1 us  [gather_from_all(): return lax.all_to_all(copies, axis, dim, dim, tiled=True)]
    all_to_all x1, waiting for transfers between devices: 0.01 us -> 13.9 us  [local(): tiles = lax.all_to_all(tiles, 'fs', 0, 0, tiled=True)]
    dot_general x14, matrix products: 13.7 us -> 20.7 us  [dot(): lax.dot_general(left, right, (((left_dim,), (right_dim,)), ((), ())), pre...]
    all_to_all x2, waiting for transfers between devices: 14.5 us -> 20.3 us  [copy_for_each(): lax.all_to_all(jnp.broadcast_to(x[None], (size, *x.shape)), axis, 0, 0, t...]
    all_to_all x0 -> x1, starting transfers between devices: none -> 5.34 us  [gather_from_all(): return lax.all_to_all(copies, axis, dim, dim, tiled=True)]
    all_to_all x2, starting transfers between devices: 14.1 us -> 9.27 us  [copy_for_each(): lax.all_to_all(jnp.broadcast_to(x[None], (size, *x.shape)), axis, 0, 0, t...]
    concatenate x2, local copies, waits for them, and re-layouts: 0.15 us -> 2.75 us  [local(): partial = jnp.concatenate([low_value.T, low_output.T], axis=1) * scale]
  transfers between devices with their start and end apart: 4 -> 5, of which waited for: 3 -> 5; matrix products, arithmetic and copies ran while one was open for 8% -> 11% of each run, Pallas kernels for 0% -> 0%
where the time goes in v1:
time: 170 us; the launch traced here: 169 us
  waiting for transfers between devices  78.6 us (46%)
  starting transfers between devices  35.6 us (21%)
  local copies, waits for them, and re-layouts  20.7 us (12%)
  matrix products  20.7 us (12%)
  other arithmetic  12 us (7%)
    all_to_all x1, waiting for transfers between devices, gather_from_all(): return lax.all_to_all(copies, axis, dim, dim, tiled=True)  37.1 us
    dot_general x14, matrix products, dot(): lax.dot_general(left, right, (((left_dim,), (right_dim,)), ((), ())), pre...  20.7 us
    all_to_all x2, waiting for transfers between devices, copy_for_each(): lax.all_to_all(jnp.broadcast_to(x[None], (size, *x.shape)), axis, 0, 0, t...  20.3 us
    all_to_all x1, starting transfers between devices, local(): tiles = lax.all_to_all(tiles, 'fs', 0, 0, tiled=True)  16.6 us
    all_to_all x1, waiting for transfers between devices, local(): tiles = lax.all_to_all(tiles, 'fs', 0, 0, tiled=True)  13.9 us
    unnamed x105, local copies, waits for them, and re-layouts  10.3 us
    all_to_all x2, starting transfers between devices, copy_for_each(): lax.all_to_all(jnp.broadcast_to(x[None], (size, *x.shape)), axis, 0, 0, t...  9.27 us
    all_to_all x1, waiting for transfers between devices, local(): pieces = lax.all_to_all(pieces, 'tp', 0, 0, tiled=True)  7.26 us
  transfers between devices with their start and end apart: 5, of which 5 were waited for; matrix products, arithmetic and copies ran while one was open for 11% of the time, Pallas kernels for 0%

profile of v1, /device:TPU:8, one launch (start us, length us, event | category | flops | bytes accessed | tf_op | source)
XLA Modules:
  0.0 169.1 jit_solution(17143054463755780011)
XLA Ops:
  0.6 0.0 copy-start
  0.7 1.2 copy-done
  1.9 1.2 convolution_bitcast_fusion.1
  3.1 0.2 copy.25
  3.3 0.0 copy-start.10
  3.3 0.0 copy-start.11
  3.3 1.2 convolution_bitcast_fusion
  4.5 0.2 copy.26
  4.7 0.9 fusion.12
  5.6 4.4 %all-to-all-start = ((f16[8,64,512]{2,1,0:T(8,128)(2,1)}), f16[8,64,512]{2,1,0:T(8,128)(2,1)}, u32[]{:S(2)}, u32[]{:S(2)}) async-start(f16[8,64,512]{2,1,0:T(8,128)(2,1)} %fusion.12), calls=%async_computation | async-start | bytes 1048576 | tf_op jit(solution)/shard_map/all_to_all | solution.py:83
  10.7 0.0 copy-start.19
  11.0 0.0 copy-done.18
  11.0 0.6 fusion.56
  11.7 0.0 copy-done.7
  11.7 0.0 copy-done.8
  11.7 1.5 multiply_reduce_fusion.1
  13.2 7.3 %all-to-all-done = f16[8,64,512]{2,1,0:T(8,128)(2,1)} async-done(((f16[8,64,512]{2,1,0:T(8,128)(2,1)}), f16[8,64,512]{2,1,0:T(8,128)(2,1)}, u32[]{:S(2)}, u32[]{:S(2)}) %all-to-all-start) | async-done | bytes 524320 | tf_op jit(solution)/shard_map/all_to_all | solution.py:83
  20.5 1.1 convert_reduce_fusion
  21.6 0.8 broadcast_in_dim.4
  22.5 4.1 %all-to-all-start.1 = ((f16[8,64,512]{2,1,0:T(8,128)(2,1)}), f16[8,64,512]{2,1,0:T(8,128)(2,1)}, u32[]{:S(2)}, u32[]{:S(2)}) async-start(f16[8,64,512]{2,1,0:T(8,128)(2,1)} %broadcast_in_dim.4), calls=%async_computation.1 | async-start | bytes 1048576 | tf_op jit(solution)/shard_map/all_to_all | solution.py:39
  26.6 3.2 %multiply_convert_fusion.1 = (bf16[512,128]{1,0:T(8,128)(2,1)}, bf16[512,128]{1,0:T(8,128)(2,1)}) fusion(f32[128]{0:T(128)S(1)} %copy-done.19, f32[512]{0:T(512)S(1)} %get-tuple-element.46, f32[]{:T(128)} %bitcast.6, bf16[512,256]{1,0:T(8,128)(2,1)S(1)} %copy-done.7, bf16[512,256]{1,0:T(8,128)(2,1)} %param.17, f32[512]{0:T(512)S(1)} %get-tuple-element.45, ...), kind=kLoop, calls=%fused_computation.41 | loop fusion | flops 917504 | bytes 791048 | tf_op jit(solution)/shard_map/convert_element_type | solution.py:49
  29.8 7.1 %all-to-all-done.1 = f16[8,64,512]{2,1,0:T(8,128)(2,1)} async-done(((f16[8,64,512]{2,1,0:T(8,128)(2,1)}), f16[8,64,512]{2,1,0:T(8,128)(2,1)}, u32[]{:S(2)}, u32[]{:S(2)}) %all-to-all-start.1) | async-done | bytes 524320 | tf_op jit(solution)/shard_map/all_to_all | solution.py:39
  36.9 1.2 fusion.11
  38.1 0.0 copy-start.5
  38.1 0.0 copy-start.6
  38.1 0.8 copy-done.5
  38.9 1.2 fusion.16
  40.2 1.0 convolution_add_fusion.2
  41.1 1.0 concatenate.45
  42.2 0.0 copy-start.14
  42.2 0.0 copy-start.15
  42.2 0.0 copy-start.16
  42.2 0.0 copy-start.17
  42.2 1.3 fusion.19
  43.5 2.0 %convolution_add_fusion.3 = f32[256,256]{1,0:T(8,128)} fusion(f32[256,256]{1,0:T(8,128)S(1)} %fusion.19, bf16[512,256]{1,0:T(8,128)(2,1)} %param.16, bf16[512,512]{1,0:T(8,128)(2,1)} %copy-done.6), kind=kOutput, calls=%fused_computation.14 | convolution fusion | flops 67174400 | bytes 1048576 | tf_op jit(solution)/shard_map/dot_general | solution.py:22
  45.5 1.7 %concatenate.43 = f32[64,4,256]{2,1,0:T(4,128)} reshape(f32[256,256]{1,0:T(8,128)} %convolution_add_fusion.3) | data formatting | bytes 524288 | tf_op jit(solution)/shard_map/concatenate | solution.py:91
  47.3 1.8 %fusion.14 = f16[64,4,512]{2,1,0:T(4,128)(2,1)} fusion(f32[64,4,256]{2,1,0:T(4,128)S(1)} %concatenate.45, f32[64,4,256]{2,1,0:T(4,128)} %concatenate.43), kind=kLoop, calls=%fused_computation.29 | loop fusion | flops 393216 | bytes 786432 | tf_op jit(solution)/shard_map/convert_element_type | solution.py:92
  49.1 16.6 %all-to-all-start.2 = ((f16[64,4,512]{2,1,0:T(4,128)(2,1)}), f16[64,4,512]{2,1,0:T(4,128)(2,1)S(1)}, u32[]{:S(2)}, u32[]{:S(2)}) async-start(f16[64,4,512]{2,1,0:T(4,128)(2,1)} %fusion.14), calls=%async_computation.2 | async-start | bytes 524288 | tf_op jit(solution)/shard_map/all_to_all | solution.py:93
  65.8 13.9 %all-to-all-done.2 = f16[64,4,512]{2,1,0:T(4,128)(2,1)S(1)} async-done(((f16[64,4,512]{2,1,0:T(4,128)(2,1)}), f16[64,4,512]{2,1,0:T(4,128)(2,1)S(1)}, u32[]{:S(2)}, u32[]{:S(2)}) %all-to-all-start.2) | async-done | bytes 262176 | tf_op jit(solution)/shard_map/all_to_all | solution.py:93
  79.7 0.1 convert_reduce_fusion.1
  79.9 0.8 broadcast_in_dim.5
  80.7 5.1 %all-to-all-start.3 = ((f16[64,4,512]{2,1,0:T(4,128)(2,1)}), f16[64,4,512]{2,1,0:T(4,128)(2,1)S(1)}, u32[]{:S(2)}, u32[]{:S(2)}) async-start(f16[64,4,512]{2,1,0:T(4,128)(2,1)} %broadcast_in_dim.5), calls=%async_computation.3 | async-start | bytes 524288 | tf_op jit(solution)/shard_map/all_to_all | solution.py:39
  85.9 0.0 copy-start.4
  85.9 13.2 %all-to-all-done.3 = f16[64,4,512]{2,1,0:T(4,128)(2,1)S(1)} async-done(((f16[64,4,512]{2,1,0:T(4,128)(2,1)}), f16[64,4,512]{2,1,0:T(4,128)(2,1)S(1)}, u32[]{:S(2)}, u32[]{:S(2)}) %all-to-all-start.3) | async-done | bytes 262176 | tf_op jit(solution)/shard_map/all_to_all | solution.py:39
  99.1 5.3 %all-to-all-start.4 = ((f16[64,32,512]{2,1,0:T(8,128)(2,1)}), f16[64,32,512]{2,1,0:T(8,128)(2,1)S(1)}, u32[]{:S(2)}, u32[]{:S(2)}) async-start(f16[64,32,512]{2,1,0:T(8,128)(2,1)} %bitcast.32), calls=%async_computation.4 | async-start | bytes 4194304 | tf_op jit(solution)/shard_map/all_to_all | solution.py:18
  104.4 0.6 fusion.54
  105.0 0.6 fusion.55
  105.6 0.9 convert_element_type.112
  106.5 2.0 %reshape.94 = f32[256,512]{1,0:T(8,128)} reshape(f32[64,4,512]{2,1,0:T(4,128)} %convert_element_type.112) | data formatting | bytes 1048576 | tf_op jit(solution)/shard_map/convert_element_type | solution.py:101
  108.5 1.2 fusion.13
  109.7 0.9 fusion.27
  110.6 0.1 fusion.33
  110.7 1.5 fusion.8
  112.2 0.8 fusion.10
  113.0 1.8 %fusion.25 = f32[256,2048]{1,0:T(8,128)} fusion(bf16[2048,256]{1,0:T(8,128)(2,1)S(1)} %copy-done.3, bf16[256,512]{1,0:T(8,128)(2,1)S(1)} %get-tuple-element.36), kind=kOutput, calls=%fused_computation.112 | convolution fusion | flops 268435456 | bytes 3276800 | tf_op jit(solution)/shard_map/dot_general | solution.py:22
  114.8 1.8 %fusion.31 = f32[256,2048]{1,0:T(8,128)} fusion(bf16[2048,256]{1,0:T(8,128)(2,1)S(1)} %copy-done, bf16[256,512]{1,0:T(8,128)(2,1)S(1)} %get-tuple-element.36), kind=kOutput, calls=%fused_computation.118 | convolution fusion | flops 268435456 | bytes 3276800 | tf_op jit(solution)/shard_map/dot_general | solution.py:22
  116.6 37.1 %all-to-all-done.4 = f16[64,32,512]{2,1,0:T(8,128)(2,1)S(1)} async-done(((f16[64,32,512]{2,1,0:T(8,128)(2,1)}), f16[64,32,512]{2,1,0:T(8,128)(2,1)S(1)}, u32[]{:S(2)}, u32[]{:S(2)}) %all-to-all-start.4) | async-done | bytes 2097184 | tf_op jit(solution)/shard_map/all_to_all | solution.py:18
  153.8 1.8 %fusion.53 = (f16[2048,256]{1,0:T(8,128)(2,1)}, f16[2048,256]{1,0:T(8,128)(2,1)}) fusion(f16[2048,512]{1,0:T(8,128)(2,1)S(1)} %bitcast.31), kind=kLoop, calls=%fused_computation.144 | loop fusion | bytes 4194304 | tf_op jit(solution)/shard_map/slice | solution.py:110
  155.5 2.7 %copy.31 = f16[2048,256]{0,1:T(8,128)(2,1)} copy(f16[2048,256]{1,0:T(8,128)(2,1)} %get-tuple-element.31) | data formatting | bytes 2097152
  158.2 2.5 %copy.30 = f16[2048,256]{0,1:T(8,128)(2,1)} copy(f16[2048,256]{1,0:T(8,128)(2,1)} %get-tuple-element.32) | data formatting | bytes 2097152
  160.7 0.0 copy-done.2
  160.7 2.8 %fusion.5 = bf16[2048,256]{0,1:T(8,128)(2,1)} fusion(f32[256,2048]{1,0:T(8,128)S(1)} %copy-done.2, bf16[2048,256]{1,0:T(8,128)(2,1)S(1)} %copy-done, f16[2048,256]{0,1:T(8,128)(2,1)} %copy.30, bf16[256,512]{1,0:T(8,128)(2,1)S(1)} %get-tuple-element.35), kind=kOutput, calls=%fused_computation.7 | convolution fusion | flops 271581184 | bytes 5373952 | tf_op jit(solution)/shard_map/dot_general | solution.py:22
  163.5 2.4 %copy.29 = bf16[2048,256]{1,0:T(8,128)(2,1)} copy(bf16[2048,256]{0,1:T(8,128)(2,1)} %fusion.5) | data formatting | bytes 2097152
  165.9 3.1 %fusion.6 = bf16[256,2048]{1,0:T(8,128)(2,1)} fusion(f32[256,2048]{1,0:T(8,128)S(1)} %copy-done.1, bf16[2048,256]{1,0:T(8,128)(2,1)} %param.23, f16[2048,256]{0,1:T(8,128)(2,1)} %copy.31, bf16[256,512]{1,0:T(8,128)(2,1)S(1)} %get-tuple-element.35), kind=kOutput, calls=%fused_computation.8 | convolution fusion | flops 271581184 | bytes 5373952 | tf_op jit(solution)/shard_map/dot_general | solution.py:22
  (90 shorter events, 0.8 us)
Async XLA Ops:
  0.6 1.2 copy-start
  0.6 2.6 %copy-start.9 = (bf16[512,256]{1,0:T(8,128)(2,1)S(1)}, bf16[512,256]{1,0:T(8,128)(2,1)}, u32[]{:S(2)}) copy-start(bf16[512,256]{1,0:T(8,128)(2,1)} %param.21) | copy-start | bytes 786436
  3.3 6.7 %copy-start.10 = (f32[256,32]{0,1:T(8,128)S(1)}, f32[256,32]{0,1:T(8,128)}, u32[]{:S(2)}) copy-start(f32[256,32]{0,1:T(8,128)} %param.25) | copy-start | bytes 98308
  3.3 6.7 %copy-start.11 = (f32[32,256]{1,0:T(8,128)S(1)}, f32[32,256]{1,0:T(8,128)}, u32[]{:S(2)}) copy-start(f32[32,256]{1,0:T(8,128)} %param.24) | copy-start | bytes 98308
  5.6 5.4 %copy-start.18 = (f32[2]{0:T(128)S(1)}, f32[2]{0:T(128)}, u32[]{:S(2)}) copy-start(f32[2]{0:T(128)} %param.19) | copy-start | bytes 28
  5.6 6.1 %copy-start.7 = (bf16[512,256]{1,0:T(8,128)(2,1)S(1)}, bf16[512,256]{1,0:T(8,128)(2,1)}, u32[]{:S(2)}) copy-start(bf16[512,256]{1,0:T(8,128)(2,1)} %param.18) | copy-start | bytes 786436
  5.6 14.9 %all-to-all-start = ((f16[8,64,512]{2,1,0:T(8,128)(2,1)}), f16[8,64,512]{2,1,0:T(8,128)(2,1)}, u32[]{:S(2)}, u32[]{:S(2)}) async-start(f16[8,64,512]{2,1,0:T(8,128)(2,1)} %fusion.12), calls=%async_computation | async-start | bytes 1048576 | tf_op jit(solution)/shard_map/all_to_all | solution.py:83
  10.0 1.6 copy-start.8
  10.7 15.9 %copy-start.19 = (f32[128]{0:T(128)S(1)}, f32[128]{0:T(128)}, u32[]{:S(2)}) copy-start(f32[128]{0:T(128)} %param.20) | copy-start | bytes 1540
  22.5 14.5 %all-to-all-start.1 = ((f16[8,64,512]{2,1,0:T(8,128)(2,1)}), f16[8,64,512]{2,1,0:T(8,128)(2,1)}, u32[]{:S(2)}, u32[]{:S(2)}) async-start(f16[8,64,512]{2,1,0:T(8,128)(2,1)} %broadcast_in_dim.4), calls=%async_computation.1 | async-start | bytes 1048576 | tf_op jit(solution)/shard_map/all_to_all | solution.py:39
  29.8 10.4 %copy-start.12 = (bf16[512,128]{1,0:T(8,128)(2,1)S(1)}, bf16[512,128]{1,0:T(8,128)(2,1)}, u32[]{:S(2)}) copy-start(bf16[512,128]{1,0:T(8,128)(2,1)} %get-tuple-element.33) | copy-start | bytes 393220
  29.8 10.4 %copy-start.13 = (bf16[512,128]{1,0:T(8,128)(2,1)S(1)}, bf16[512,128]{1,0:T(8,128)(2,1)}, u32[]{:S(2)}) copy-start(bf16[512,128]{1,0:T(8,128)(2,1)} %get-tuple-element.34) | copy-start | bytes 393220
  38.1 0.8 copy-start.5
  38.1 2.0 %copy-start.6 = (bf16[512,512]{1,0:T(8,128)(2,1)}, bf16[512,512]{1,0:T(8,128)(2,1)S(1)}, u32[]{:S(2)}) copy-start(bf16[512,512]{1,0:T(8,128)(2,1)S(1)} %get-tuple-element.37) | copy-start | bytes 1572868
  42.2 37.7 %copy-start.14 = (f32[4,256]{1,0:T(4,128)S(1)}, f32[4,256]{1,0:T(4,128)}, u32[]{:S(2)}) copy-start(f32[4,256]{1,0:T(4,128)} %param.29) | copy-start | bytes 12292
  42.2 37.6 %copy-start.15 = (f32[4,256]{1,0:T(4,128)S(1)}, f32[4,256]{1,0:T(4,128)}, u32[]{:S(2)}) copy-start(f32[4,256]{1,0:T(4,128)} %param.27) | copy-start | bytes 12292
  42.2 37.6 %copy-start.16 = (f32[4,256]{1,0:T(4,128)S(1)}, f32[4,256]{1,0:T(4,128)}, u32[]{:S(2)}) copy-start(f32[4,256]{1,0:T(4,128)} %param.28) | copy-start | bytes 12292
  42.2 37.6 %copy-start.17 = (f32[4,256]{1,0:T(4,128)S(1)}, f32[4,256]{1,0:T(4,128)}, u32[]{:S(2)}) copy-start(f32[4,256]{1,0:T(4,128)} %param.26) | copy-start | bytes 12292
  49.1 30.6 %all-to-all-start.2 = ((f16[64,4,512]{2,1,0:T(4,128)(2,1)}), f16[64,4,512]{2,1,0:T(4,128)(2,1)S(1)}, u32[]{:S(2)}, u32[]{:S(2)}) async-start(f16[64,4,512]{2,1,0:T(4,128)(2,1)} %fusion.14), calls=%async_computation.2 | async-start | bytes 524288 | tf_op jit(solution)/shard_map/all_to_all | solution.py:93
  80.7 18.4 %all-to-all-start.3 = ((f16[64,4,512]{2,1,0:T(4,128)(2,1)}), f16[64,4,512]{2,1,0:T(4,128)(2,1)S(1)}, u32[]{:S(2)}, u32[]{:S(2)}) async-start(f16[64,4,512]{2,1,0:T(4,128)(2,1)} %broadcast_in_dim.5), calls=%async_computation.3 | async-start | bytes 524288 | tf_op jit(solution)/shard_map/all_to_all | solution.py:39
  85.9 13.2 %copy-start.4 = (f16[2048,512]{1,0:T(8,128)(2,1)}, f16[2048,512]{1,0:T(8,128)(2,1)S(1)}, u32[]{:S(2)}) copy-start(f16[2048,512]{1,0:T(8,128)(2,1)S(1)} %constant_dynamic-update-slice_fusion) | copy-start | bytes 6291460
  99.1 54.7 %all-to-all-start.4 = ((f16[64,32,512]{2,1,0:T(8,128)(2,1)}), f16[64,32,512]{2,1,0:T(8,128)(2,1)S(1)}, u32[]{:S(2)}, u32[]{:S(2)}) async-start(f16[64,32,512]{2,1,0:T(8,128)(2,1)} %bitcast.32), calls=%async_computation.4 | async-start | bytes 4194304 | tf_op jit(solution)/shard_map/all_to_all | solution.py:18
  108.5 4.5 %copy-start.3 = (bf16[2048,256]{1,0:T(8,128)(2,1)S(1)}, bf16[2048,256]{1,0:T(8,128)(2,1)}, u32[]{:S(2)}) copy-start(bf16[2048,256]{1,0:T(8,128)(2,1)} %param.23) | copy-start | bytes 3145732
  155.5 5.2 %copy-start.2 = (f32[256,2048]{1,0:T(8,128)S(1)}, f32[256,2048]{1,0:T(8,128)}, u32[]{:S(2)}) copy-start(f32[256,2048]{1,0:T(8,128)} %fusion.31) | copy-start | bytes 6291460
  163.5 2.4 %copy-start.1 = (f32[256,2048]{1,0:T(8,128)S(1)}, f32[256,2048]{1,0:T(8,128)}, u32[]{:S(2)}) copy-start(f32[256,2048]{1,0:T(8,128)} %fusion.25) | copy-start | bytes 6291460
